TPU v7x, 32 devices: a whole 2x2x4 slice. The times are simulated.
32 devices in a mesh: sp: 8 (over z, y), tp: 4 (over x, core).
Axes of the slice: x: 2, y: 2, z: 4, core: 2. Of those that a mesh axis runs over, the one named last changes fastest.
Arguments:
- resid: bfloat16 [2048, 2048], P(('sp', 'tp')), may hold values from -6 to 6
- query_a: bfloat16 [2048, 4, 128], P('sp', 'tp')
- key_a: bfloat16 [2048, 4, 128], P('sp', 'tp')
- value_a: bfloat16 [2048, 4, 128], P('sp', 'tp'), may hold values from -6 to 6
- query_b: bfloat16 [2048, 4, 256], P('sp', 'tp')
- key_b: bfloat16 [2048, 4, 256], P('sp', 'tp')
- value_b: bfloat16 [2048, 4, 128], P('sp', 'tp'), may hold values from -6 to 6
- lambda_a: float32 [4], P('tp'), may hold values from 0.3 to 0.8
- lambda_b: float32 [4], P('tp'), may hold values from 0.3 to 0.8
- head_gain: float32 [128], replicated, may hold values from 0.1 to 1.9
- out_weight: bfloat16 [1024, 2048], replicated, may hold values from -0.1875 to 0.1875
- norm_gain: float32 [2048], replicated, may hold values from 0.1 to 1.9
- expert_ids: int32 [2048, 4], P(('sp', 'tp')), may hold values from 0 to 31, all different within a row; in each aligned block of 64 rows (0 to 63, 64 to 127, ...) at most 16 rows name the same one
- expert_mix: float32 [2048, 4], P(('sp', 'tp')), may hold values from 0.2 to 1
- gate_experts: bfloat16 [32, 2048, 1024], P(('sp', 'tp')), may hold values from -0.125 to 0.125
- up_experts: bfloat16 [32, 2048, 1024], P(('sp', 'tp')), may hold values from -0.125 to 0.125
- down_experts: bfloat16 [32, 1024, 2048], P(('sp', 'tp')), may hold values from -0.1875 to 0.1875
- shared_gate: bfloat16 [2048, 512], replicated, may hold values from -0.125 to 0.125
- shared_up: bfloat16 [2048, 512], replicated, may hold values from -0.125 to 0.125
- shared_down: bfloat16 [512, 2048], replicated, may hold values from -0.25 to 0.25
Outputs:
- layer_out: bfloat16 [2048, 2048], P(('sp', 'tp'))
Inputs may be any that keep to these rules, and one draw needn't show every extreme that they name: `expert_ids`: in each aligned block of 64 rows (the rows of one device) no expert is named more than 16 times, a bound that some block reaches.
All inputs are finite; a program needn't handle non-finite values.
Results may differ from a plain program's by a relative error of at most 0.017.
Values may be sent and summed in bfloat16 or wider, within the bound.
A program may use at most 128 MiB of HBM per device.

v0:
```python
import math

import jax
import jax.numpy as jnp
from jax import lax
from jax.sharding import PartitionSpec as P

NEG_FILL = -1e30
EPSILON = 1e-05
HEAD_SCALE = 0.8
KEY_SPAN = 2048


def swiglu_rows(row_set, w_gate, w_up, w_down):
    gate_val = jnp.dot(row_set, w_gate, preferred_element_type=jnp.float32)
    up_val = jnp.dot(row_set, w_up, preferred_element_type=jnp.float32)
    hidden = (jax.nn.silu(gate_val) * up_val).astype(jnp.bfloat16)
    return jnp.dot(hidden, w_down, preferred_element_type=jnp.float32)


def online_update(state, query_map, key_map, value_block, causal, scaling):
    row_top, denoms, numerator = state
    scores = (
        jnp.einsum("qhd,khd->hqk", query_map, key_map, preferred_element_type=jnp.float32) * scaling
    )
    scores = jnp.where(causal, scores, NEG_FILL)
    new_top = jnp.maximum(row_top, jnp.max(scores, axis=2))
    exponent = jnp.where(causal, jnp.exp(scores - new_top[:, :, None]), 0.0)
    shrink = jnp.exp(row_top - new_top)
    denoms = denoms * shrink + jnp.sum(exponent, axis=2)
    numerator = numerator * jnp.transpose(shrink)[:, :, None] + jnp.einsum(
        "hqk,khe->qhe",
        exponent.astype(jnp.bfloat16),
        value_block,
        preferred_element_type=jnp.float32,
    )
    return (new_top, denoms, numerator)


def group_update(states, queries, key_block, value_block, causal):
    map_width = queries.shape[2] // 2
    scaling = map_width ** (-0.5)
    first_state = online_update(
        states[0],
        queries[:, :, :map_width],
        key_block[:, :, :map_width],
        value_block,
        causal,
        scaling,
    )
    second_state = online_update(
        states[1],
        queries[:, :, map_width:],
        key_block[:, :, map_width:],
        value_block,
        causal,
        scaling,
    )
    return (first_state, second_state)


def empty_state(query_rows, head_count, value_width):
    single = (
        jnp.full((head_count, query_rows), NEG_FILL, jnp.float32),
        jnp.zeros((head_count, query_rows), jnp.float32),
        jnp.zeros((query_rows, head_count, value_width), jnp.float32),
    )
    return (single, single)


def finish_group(states, lambdas, head_gain):
    first_out = states[0][2] / jnp.transpose(states[0][1])[:, :, None]
    second_out = states[1][2] / jnp.transpose(states[1][1])[:, :, None]
    differ = first_out - lambdas[None, :, None] * second_out
    scale_rms = lax.rsqrt(jnp.mean(differ * differ, axis=2, keepdims=True) + EPSILON)
    return (differ * scale_rms * head_gain[None, None, :] * HEAD_SCALE).astype(jnp.bfloat16)


def per_device(
    resid,
    query_a,
    key_a,
    value_a,
    query_b,
    key_b,
    value_b,
    lambda_a,
    lambda_b,
    head_gain,
    out_weight,
    norm_gain,
    expert_ids,
    expert_mix,
    gate_experts,
    up_experts,
    down_experts,
    shared_gate,
    shared_up,
    shared_down,
):
    query_rows = query_a.shape[0]
    value_width = value_a.shape[2]
    query_pos = lax.axis_index("sp") * query_rows + jnp.arange(query_rows, dtype=jnp.int32)
    start_state = (
        empty_state(query_rows, query_a.shape[1], value_width),
        empty_state(query_rows, query_b.shape[1], value_width),
    )
    key_piece_a = lax.all_gather(key_a, "sp", axis=0, tiled=True)
    value_piece_a = lax.all_gather(value_a, "sp", axis=0, tiled=True)
    key_piece_b = lax.all_gather(key_b, "sp", axis=0, tiled=True)
    value_piece_b = lax.all_gather(value_b, "sp", axis=0, tiled=True)
    piece_rows = key_piece_a.shape[0]
    step_rows = math.gcd(piece_rows, KEY_SPAN)

    def one_step(step_index, inner_state):
        begin_row = step_index * step_rows
        key_pos = begin_row + jnp.arange(step_rows, dtype=jnp.int32)
        causal = (key_pos[None, :] <= query_pos[:, None])[None]
        part_a = group_update(
            inner_state[0],
            query_a,
            lax.dynamic_slice_in_dim(key_piece_a, begin_row, step_rows, 0),
            lax.dynamic_slice_in_dim(value_piece_a, begin_row, step_rows, 0),
            causal,
        )
        part_b = group_update(
            inner_state[1],
            query_b,
            lax.dynamic_slice_in_dim(key_piece_b, begin_row, step_rows, 0),
            lax.dynamic_slice_in_dim(value_piece_b, begin_row, step_rows, 0),
            causal,
        )
        return (part_a, part_b)

    state_a, state_b = lax.fori_loop(0, piece_rows // step_rows, one_step, start_state)
    heads_a = finish_group(state_a, lambda_a, head_gain)
    heads_b = finish_group(state_b, lambda_b, head_gain)
    tok_dev = resid.shape[0]
    back_a, back_b = (
        lax.all_to_all(heads_a, "tp", split_axis=0, concat_axis=1, tiled=True),
        lax.all_to_all(heads_b, "tp", split_axis=0, concat_axis=1, tiled=True),
    )
    joined = jnp.concatenate([back_a.reshape(tok_dev, -1), back_b.reshape(tok_dev, -1)], axis=1)
    project = jnp.dot(joined, out_weight, preferred_element_type=jnp.float32)
    middle = (resid.astype(jnp.float32) + project).astype(jnp.bfloat16)
    middle_f = middle.astype(jnp.float32)
    normed = (
        middle_f
        * lax.rsqrt(jnp.mean(middle_f * middle_f, axis=1, keepdims=True) + EPSILON)
        * norm_gain[None, :]
    ).astype(jnp.bfloat16)
    shared = swiglu_rows(normed, shared_gate, shared_up, shared_down)
    top_count = expert_ids.shape[1]
    model_width = normed.shape[1]
    sp_count = lax.axis_size("sp")
    tp_count = lax.axis_size("tp")
    expert_total = sp_count * tp_count
    pair_count = tok_dev * top_count
    capacity = max(2, 2 * pair_count // expert_total)
    flat_ids = expert_ids.reshape(-1)
    one_hot = (flat_ids[:, None] == jnp.arange(expert_total, dtype=jnp.int32)[None, :]).astype(
        jnp.int32
    )
    pair_rank = jnp.sum((jnp.cumsum(one_hot, axis=0) - one_hot) * one_hot, axis=1)
    pair_token = jnp.arange(pair_count, dtype=jnp.int32) // top_count
    send_rows = (
        jnp.zeros((expert_total, capacity, model_width), jnp.bfloat16)
        .at[flat_ids, pair_rank]
        .set(normed[pair_token])
    )
    arrived = lax.all_to_all(send_rows, ("sp", "tp"), split_axis=0, concat_axis=0, tiled=True)
    arrived_shape = arrived.shape
    flat_rows = arrived.reshape(-1, arrived_shape[-1])
    result = swiglu_rows(flat_rows, gate_experts[0], up_experts[0], down_experts[0]).astype(
        jnp.bfloat16
    )
    finished = result.reshape(arrived_shape)
    returned = lax.all_to_all(finished, ("sp", "tp"), split_axis=0, concat_axis=0, tiled=True)
    chosen = returned[flat_ids, pair_rank].reshape(tok_dev, top_count, model_width)
    routed = jnp.sum(chosen.astype(jnp.float32) * expert_mix[:, :, None], axis=1)
    return (middle_f + shared + routed).astype(jnp.bfloat16)


def solution(mesh):
    in_specs = (
        P(("sp", "tp"), None),
        P("sp", "tp", None),
        P("sp", "tp", None),
        P("sp", "tp", None),
        P("sp", "tp", None),
        P("sp", "tp", None),
        P("sp", "tp", None),
        P("tp"),
        P("tp"),
        P(),
        P(),
        P(),
        P(("sp", "tp"), None),
        P(("sp", "tp"), None),
        P(("sp", "tp"), None, None),
        P(("sp", "tp"), None, None),
        P(("sp", "tp"), None, None),
        P(),
        P(),
        P(),
    )
    out_specs = P(("sp", "tp"), None)
    return jax.shard_map(
        per_device, mesh=mesh, in_specs=in_specs, out_specs=out_specs, check_vma=False
    )
```

profile of v0, /device:TPU:0, one launch (start us, length us, event | category | flops | bytes accessed | tf_op | source)
XLA Modules:
  0.0 333.9 jit_solution(18437636033774966400)
XLA Ops:
  6.5 0.0 copy-start
  6.5 0.0 all-gather.2.cloned.1.call-start
  6.5 0.7 all-gather.2.cloned.1.call-update
  7.3 33.6 %all_gather.12 = bf16[2048,1,128]{2,0,1:T(8,128)(2,1)S(1)} all-gather(bf16[256,1,128]{2,0,1:T(8,128)(2,1)} %param.22), channel_id=1, replica_groups=mesh['sp'=8,'tp'=4] {'sp'}, dimensions={0}, use_global_device_ids=true | all-gather | bytes 589824 | tf_op jit(solution)/shard_map/all_gather | solution.py:108
  40.9 0.8 copy.35
  41.6 0.1 eq.29
  41.8 0.6 reduce-window.6
  42.4 0.2 slice_reduce_fusion
  42.6 0.1 eq.25
  42.7 0.1 reshape.406
  44.1 0.1 fusion.73
  44.2 2.8 fusion.88
  47.0 0.0 copy-done.12
  47.0 0.0 copy-start.11
  47.0 1.8 fusion.89
  48.9 0.0 copy-done.5
  48.9 31.4 %all_gather.15 = bf16[2048,1,128]{2,0,1:T(8,128)(2,1)S(1)} all-gather(bf16[256,1,128]{2,0,1:T(8,128)(2,1)S(1)} %copy-done.5), channel_id=1, replica_groups=mesh['sp'=8,'tp'=4] {'sp'}, dimensions={0}, use_global_device_ids=true | all-gather | bytes 589824 | tf_op jit(solution)/shard_map/all_gather | solution.py:111
  80.3 0.0 copy-done.6
  80.3 31.5 %all_gather.13 = bf16[2048,1,128]{2,0,1:T(8,128)(2,1)S(1)} all-gather(bf16[256,1,128]{2,0,1:T(8,128)(2,1)S(1)} %copy-done.6), channel_id=1, replica_groups=mesh['sp'=8,'tp'=4] {'sp'}, dimensions={0}, use_global_device_ids=true | all-gather | bytes 589824 | tf_op jit(solution)/shard_map/all_gather | solution.py:109
  111.8 0.0 copy-done.11
  111.8 1.8 fusion.91
  113.6 1.8 fusion.90
  115.4 2.1 fusion.19
  117.5 0.7 fusion.38
  118.2 0.7 multiply_reduce_fusion.2
  118.9 0.7 fusion.32
  119.6 0.0 copy-start.9
  119.6 0.7 multiply_reduce_fusion.3
  120.3 0.0 copy-start.4
  120.3 0.1 fusion.60
  120.4 0.6 broadcast.531
  121.0 0.7 reduce.22
  121.7 0.1 copy.50
  121.8 0.7 reshape.432
  122.5 3.3 all-to-all-start.1
  125.8 0.7 reduce.23
  126.5 0.1 copy.51
  126.6 0.6 reshape.434
  127.3 2.6 all-to-all-done.1
  129.9 3.3 all-to-all-start
  133.2 0.1 reshape.433
  133.2 0.1 copy.34
  133.3 3.9 %all-to-all-done = bf16[4,2,4096]{2,1,0:T(2,128)(2,1)S(1)} async-done(((bf16[4,2,4096]{2,1,0:T(2,128)(2,1)}), bf16[4,2,4096]{2,1,0:T(2,128)(2,1)S(1)}, u32[]{:S(2)}, u32[]{:S(2)}) %all-to-all-start) | async-done | bytes 65568 | tf_op jit(solution)/shard_map/all_to_all | solution.py:140
  137.2 0.1 reshape.435
  137.3 0.1 copy.32
  137.4 0.0 copy-done.4
  137.4 0.0 copy-start.7
  137.4 3.2 multiply_reduce_fusion.1
  140.6 0.1 multiply_convert_fusion.1
  140.7 2.3 gather_fusion
  143.1 1.6 broadcast_in_dim.49
  144.7 46.2 %scatter_fusion = bf16[32,16,2048]{2,1,0:T(8,128)(2,1)} fusion(bf16[32,16,2048]{2,1,0:T(8,128)(2,1)} %broadcast_in_dim.49, s32[256]{0:T(256)S(1)} %bitcast.169, bf16[256,2048]{1,0:T(8,128)(2,1)} %gather_fusion), kind=kCustom, calls=%fused_computation.2 | custom fusion | bytes 3147776 | tf_op jit(solution)/shard_map/scatter | solution.py:169
  190.9 53.7 %all_to_all.40 = bf16[32,16,2048]{2,1,0:T(8,128)(2,1)S(1)} all-to-all(bf16[32,16,2048]{2,1,0:T(8,128)(2,1)} %scatter_fusion), channel_id=1, replica_groups=mesh['sp'=8,'tp'=4] {'sp','tp'}, dimensions={0} | all-to-all | bytes 4194304 | tf_op jit(solution)/shard_map/all_to_all | solution.py:171
  244.6 1.3 copy-done.3
  245.9 3.6 %fusion.4 = f32[512,1024]{1,0:T(8,128)} fusion(bf16[512,2048]{1,0:T(8,128)(2,1)S(1)} %bitcast.171, bf16[1,2048,1024]{2,1,0:T(8,128)(2,1)S(1)} %copy-done.10), kind=kOutput, calls=%fused_computation.7 | convolution fusion | flops 2147483648 | bytes 8388608 | tf_op jit(solution)/shard_map/dot_general | solution.py:15
  249.6 10.6 %fusion.6 = bf16[512,2048]{1,0:T(8,128)(2,1)} fusion(bf16[1,1024,2048]{2,1,0:T(8,128)(2,1)} %param.36, f32[512,1024]{1,0:T(8,128)} %fusion.4, bf16[512,2048]{1,0:T(8,128)(2,1)} %bitcast.172, bf16[1,2048,1024]{2,1,0:T(8,128)(2,1)} %param.35), kind=kOutput, calls=%fused_computation.9 | convolution fusion | flops 4299161600 | bytes 14680064 | tf_op jit(solution)/shard_map/dot_general | solution.py:18
  260.2 3.8 %all-to-all-start.3 = ((bf16[32,16,2048]{2,1,0:T(8,128)(2,1)}), bf16[32,16,2048]{2,1,0:T(8,128)(2,1)}, u32[]{:S(2)}, u32[]{:S(2)}) async-start(bf16[32,16,2048]{2,1,0:T(8,128)(2,1)} %bitcast.170), calls=%async_computation.3 | async-start | bytes 4194304 | tf_op jit(solution)/shard_map/all_to_all | solution.py:178
  264.0 0.7 copy.39
  264.7 2.1 fusion.92
  266.8 45.9 %all-to-all-done.3 = bf16[32,16,2048]{2,1,0:T(8,128)(2,1)} async-done(((bf16[32,16,2048]{2,1,0:T(8,128)(2,1)}), bf16[32,16,2048]{2,1,0:T(8,128)(2,1)}, u32[]{:S(2)}, u32[]{:S(2)}) %all-to-all-start.3) | async-done | bytes 2097184 | tf_op jit(solution)/shard_map/all_to_all | solution.py:178
  312.7 5.1 %gather_fusion.1 = bf16[256,2048]{1,0:T(8,128)(2,1)} fusion(bf16[32,16,2048]{2,1,0:T(8,128)(2,1)} %all-to-all-done.3, s32[256]{0:T(256)S(1)} %bitcast.168), kind=kCustom, calls=%fused_computation.1 | custom fusion | bytes 2099200 | tf_op jit(solution)/shard_map/gather | solution.py:179
  317.8 2.7 reshape.410
  320.6 3.2 multiply_reduce_fusion
  323.8 3.2 fusion.14
  (36 shorter events, 0.2 us)
Async XLA Ops:
  6.5 317.3 %copy-start = (bf16[512,2048]{1,0:T(8,128)(2,1)S(1)}, bf16[512,2048]{1,0:T(8,128)(2,1)}, u32[]{:S(2)}) copy-start(bf16[512,2048]{1,0:T(8,128)(2,1)} %param.39) | copy-start | bytes 6291460
  6.5 40.5 %copy-start.12 = (bf16[256,1,128]{2,0,1:T(8,128)(2,1)S(1)}, bf16[256,1,128]{2,0,1:T(8,128)(2,1)}, u32[]{:S(2)}) copy-start(bf16[256,1,128]{2,0,1:T(8,128)(2,1)} %param.21) | copy-start | bytes 196612
  6.5 105.2 %all-gather.2.cloned.1.call-start = ((), (), s32[]{:S(2)}) async-start(), calls=%async_computation.4 | async-start | bytes 1179648 | tf_op jit(solution)/shard_map/all_gather | solution.py:110
  47.0 1.9 copy-start.5
  47.0 33.3 %copy-start.6 = (bf16[256,1,128]{2,0,1:T(8,128)(2,1)S(1)}, bf16[256,1,128]{2,0,1:T(8,128)(2,1)}, u32[]{:S(2)}) copy-start(bf16[256,1,128]{2,0,1:T(8,128)(2,1)} %param.23) | copy-start | bytes 196612
  47.0 64.8 %copy-start.11 = (bf16[256,1,256]{2,0,1:T(8,128)(2,1)S(1)}, bf16[256,1,256]{2,0,1:T(8,128)(2,1)}, u32[]{:S(2)}) copy-start(bf16[256,1,256]{2,0,1:T(8,128)(2,1)} %param.24) | copy-start | bytes 393220
  111.8 3.6 %copy-start.2 = (f32[256,2048]{1,0:T(8,128)S(1)}, f32[256,2048]{1,0:T(8,128)}, u32[]{:S(2)}) copy-start(f32[256,2048]{1,0:T(8,128)} %get-tuple-element.62) | copy-start | bytes 6291460
  113.6 1.8 copy-start.1
  119.6 0.7 copy-start.9
  120.3 17.1 %copy-start.4 = (bf16[64,2048]{1,0:T(8,128)(2,1)S(1)}, bf16[64,2048]{1,0:T(8,128)(2,1)}, u32[]{:S(2)}) copy-start(bf16[64,2048]{1,0:T(8,128)(2,1)} %param.20) | copy-start | bytes 786436
  122.5 7.4 %all-to-all-start.1 = ((bf16[4,2,4096]{2,1,0:T(2,128)(2,1)}), bf16[4,2,4096]{2,1,0:T(2,128)(2,1)S(1)}, u32[]{:S(2)}, u32[]{:S(2)}) async-start(bf16[4,2,4096]{2,1,0:T(2,128)(2,1)} %reshape.432), calls=%async_computation.1 | async-start | bytes 131072 | tf_op jit(solution)/shard_map/all_to_all | solution.py:141
  129.9 7.4 %all-to-all-start = ((bf16[4,2,4096]{2,1,0:T(2,128)(2,1)}), bf16[4,2,4096]{2,1,0:T(2,128)(2,1)S(1)}, u32[]{:S(2)}, u32[]{:S(2)}) async-start(bf16[4,2,4096]{2,1,0:T(2,128)(2,1)} %reshape.434), calls=%async_computation | async-start | bytes 131072 | tf_op jit(solution)/shard_map/all_to_all | solution.py:140
  137.4 3.2 copy-start.7
  190.9 55.0 %copy-start.10 = (bf16[1,2048,1024]{2,1,0:T(8,128)(2,1)S(1)}, bf16[1,2048,1024]{2,1,0:T(8,128)(2,1)}, u32[]{:S(2)}) copy-start(bf16[1,2048,1024]{2,1,0:T(8,128)(2,1)} %param.34) | copy-start | bytes 12582916
  244.6 1.3 copy-start.3
  260.2 3.8 %copy-start.8 = (f32[64,4]{0,1:T(4,128)S(1)}, f32[64,4]{0,1:T(4,128)}, u32[]{:S(2)}) copy-start(f32[64,4]{0,1:T(4,128)} %param.33) | copy-start | bytes 3076
  260.2 52.5 %all-to-all-start.3 = ((bf16[32,16,2048]{2,1,0:T(8,128)(2,1)}), bf16[32,16,2048]{2,1,0:T(8,128)(2,1)}, u32[]{:S(2)}, u32[]{:S(2)}) async-start(bf16[32,16,2048]{2,1,0:T(8,128)(2,1)} %bitcast.170), calls=%async_computation.3 | async-start | bytes 4194304 | tf_op jit(solution)/shard_map/all_to_all | solution.py:178
Sparse Core Ops, SparseCore 0:
  9.5 43.6 all-gather.1
where the time goes:
time: 336 us; the launch traced here: 334 us
  blocking collectives  150 us (45%)
  local copies, waits for them, and re-layouts  63.8 us (19%)
  waiting for transfers between devices  53.1 us (16%)
  matrix products  33.6 us (10%)
  between operations  15.1 us (4%)
  starting transfers between devices  10.4 us (3%)
  other arithmetic  7.7 us (2%)
    all_to_all x1, blocking collectives, per_device(): lax.all_to_all(send_rows, ('sp', 'tp'), split_axis=0, concat_axis=0, tile...  53.7 us
    scatter x1, local copies, waits for them, and re-layouts, per_device(): send_rows = jnp.zeros((expert_total, capacity, model_width), jnp.bfloat16...  46.2 us
    all_to_all x1, waiting for transfers between devices, per_device(): lax.all_to_all(finished, ('sp', 'tp'), split_axis=0, concat_axis=0, tiled...  45.9 us
    all_gather x1, blocking collectives, per_device(): key_piece_a = lax.all_gather(key_a, 'sp', axis=0, tiled=True)  33.6 us
    all_gather x1, blocking collectives, per_device(): value_piece_a = lax.all_gather(value_a, 'sp', axis=0, tiled=True)  31.5 us
    all_gather x1, blocking collectives, per_device(): value_piece_b = lax.all_gather(value_b, 'sp', axis=0, tiled=True)  31.4 us
    dot_general x2, matrix products, swiglu_rows(): return jnp.dot(hidden, w_down, preferred_element_type=jnp.float32)  13.8 us
    dot_general x4, matrix products, online_update(): jnp.einsum('qhd,khd->hqk', query_map, key_map, preferred_element_type=jnp...  8.17 us
  transfers between devices with their start and end apart: 4, of which 3 were waited for; matrix products, arithmetic and copies ran while one was open for 3% of the time, Pallas kernels for 0%

commit v1 on v0

v1 whole, which is shorter than its diff:
```python
import functools
import math

import jax
import jax.numpy as jnp
from jax import lax
from jax.experimental import pallas as pl
from jax.experimental.pallas import tpu as pltpu
from jax.sharding import PartitionSpec as P

NEG_FILL = -1e30
EPSILON = 1e-05
HEAD_SCALE = 0.8
MESH = pl.DeviceIdType.MESH


def swiglu_rows(row_set, w_gate, w_up, w_down):
    gate_val = jnp.dot(row_set, w_gate, preferred_element_type=jnp.float32)
    up_val = jnp.dot(row_set, w_up, preferred_element_type=jnp.float32)
    hidden = (jax.nn.silu(gate_val) * up_val).astype(jnp.bfloat16)
    return jnp.dot(hidden, w_down, preferred_element_type=jnp.float32)


def attention_kernel(
    sp_count,
    tp_count,
    scalings,
    query_a,
    query_b,
    local_a,
    local_b,
    lam_a,
    lam_b,
    gain,
    joined,
    kv_a,
    kv_b,
    tops,
    sums,
    numers,
    heads,
    send_z,
    send_y,
    recv,
    send_t,
    recv_t,
):
    sp = lax.axis_index("sp")
    tp = lax.axis_index("tp")
    chain = sp_count // 2
    spot = sp // 2
    side = sp % 2
    other = spot * 2 + (1 - side)
    rows = local_a.shape[0]
    part = rows // tp_count
    width = gain.shape[1]
    stores = (kv_a, kv_b)
    queries = (query_a, query_b)

    barrier = pltpu.get_barrier_semaphore()

    @pl.when(spot > 0)
    def _():
        pl.semaphore_signal(barrier, inc=1, device_id=(sp - 2, tp), device_id_type=MESH)

    @pl.when(spot < chain - 1)
    def _():
        pl.semaphore_signal(barrier, inc=1, device_id=(sp + 2, tp), device_id_type=MESH)

    pl.semaphore_signal(barrier, inc=1, device_id=(other, tp), device_id_type=MESH)
    for step in range(1, tp_count):
        peer = (tp + step) % tp_count
        pl.semaphore_signal(barrier, inc=1, device_id=(sp, peer), device_id_type=MESH)

    kv_a[sp] = local_a[...]
    kv_b[sp] = local_b[...]
    tops[...] = jnp.full(tops.shape, NEG_FILL, jnp.float32)
    sums[...] = jnp.zeros(sums.shape, jnp.float32)
    numers[...] = jnp.zeros(numers.shape, jnp.float32)
    linked = jnp.where(spot > 0, 1, 0) + jnp.where(spot < chain - 1, 1, 0) + tp_count
    pl.semaphore_wait(barrier, linked)

    def along(block, group, source):
        return pltpu.make_async_remote_copy(
            src_ref=source,
            dst_ref=stores[group].at[block],
            send_sem=send_z.at[block, group],
            recv_sem=recv.at[block, group],
            device_id=(sp + 2, tp),
            device_id_type=MESH,
        )

    def across(block, group, source):
        return pltpu.make_async_remote_copy(
            src_ref=source,
            dst_ref=stores[group].at[block],
            send_sem=send_y.at[block, group],
            recv_sem=recv.at[block, group],
            device_id=(other, tp),
            device_id_type=MESH,
        )

    def attend(block, group):
        store = stores[group]
        query = queries[group]
        key_width = store.shape[2] - width
        base = (sp - block) * rows
        row_at = lax.broadcasted_iota(jnp.int32, (rows, rows), 0)
        col_at = lax.broadcasted_iota(jnp.int32, (rows, rows), 1)
        causal = col_at <= row_at + base
        value = store[block, :, key_width:]
        for index in range(2):
            at = group * 2 + index
            if query.shape[2] == key_width:
                key = store[block, :, :key_width]
            else:
                half = key_width // 2
                key = store[block, :, index * half : (index + 1) * half]
            scores = (
                lax.dot_general(
                    query[index],
                    key,
                    (((1,), (1,)), ((), ())),
                    preferred_element_type=jnp.float32,
                )
                * scalings[group]
            )
            scores = jnp.where(causal, scores, NEG_FILL)
            old_top = tops[at][:, :1]
            new_top = jnp.maximum(old_top, jnp.max(scores, axis=1, keepdims=True))
            exponent = jnp.where(causal, jnp.exp(scores - new_top), 0.0)
            shrink = jnp.exp(old_top - new_top)
            total = sums[at][:, :1] * shrink + jnp.sum(exponent, axis=1, keepdims=True)
            tops[at] = jnp.broadcast_to(new_top, tops.shape[1:])
            sums[at] = jnp.broadcast_to(total, sums.shape[1:])
            numers[at] = numers[at] * shrink + jnp.dot(
                exponent.astype(jnp.bfloat16), value, preferred_element_type=jnp.float32
            )

    locals_ = (local_a, local_b)
    for group in range(2):

        @pl.when(spot < chain - 1)
        def _():
            along(sp, group, locals_[group]).start()

        @pl.when(side == 0)
        def _():
            across(sp, group, locals_[group]).start()

    for group in range(2):
        attend(sp, group)

    @pl.when(side == 1)
    def _():
        for group in range(2):
            across(other, group, stores[group].at[other]).wait_recv()
            attend(other, group)

    @pl.loop(1, chain)
    def _(back):
        @pl.when(back <= spot)
        def _():
            mine = sp - 2 * back
            theirs = other - 2 * back
            for group in range(2):
                along(mine, group, stores[group].at[mine]).wait_recv()

                @pl.when(spot < chain - 1)
                def _():
                    along(mine, group, stores[group].at[mine]).start()

                across(mine, group, stores[group].at[mine]).start()
            for group in range(2):
                attend(mine, group)
            for group in range(2):
                across(theirs, group, stores[group].at[theirs]).wait_recv()
                attend(theirs, group)

    lams = (lam_a, lam_b)
    for group in range(2):
        first = numers[2 * group] / sums[2 * group][:, :1]
        second = numers[2 * group + 1] / sums[2 * group + 1][:, :1]
        differ = first - lams[group][0] * second
        scale_rms = lax.rsqrt(jnp.mean(differ * differ, axis=1, keepdims=True) + EPSILON)
        heads[:, group * width : (group + 1) * width] = (
            differ * scale_rms * gain[...] * HEAD_SCALE
        ).astype(jnp.bfloat16)

    def columns(who, group):
        return pl.ds(pl.multiple_of((group * tp_count + who) * width, width), width)

    def spread(step, group):
        peer = (tp + step) % tp_count
        start = pl.multiple_of(peer * part, part)
        return pltpu.make_async_remote_copy(
            src_ref=heads.at[pl.ds(start, part), group * width : (group + 1) * width],
            dst_ref=joined.at[:, columns(tp, group)],
            send_sem=send_t.at[step, group],
            recv_sem=recv_t.at[step, group],
            device_id=(sp, peer),
            device_id_type=MESH,
        )

    for step in range(1, tp_count):
        for group in range(2):
            spread(step, group).start()
    own = pl.multiple_of(tp * part, part)
    for group in range(2):
        joined[:, columns(tp, group)] = heads[
            pl.ds(own, part), group * width : (group + 1) * width
        ]

    for group in range(2):

        @pl.when(spot < chain - 1)
        def _():
            along(sp, group, locals_[group]).wait_send()

        @pl.when(side == 0)
        def _():
            across(sp, group, locals_[group]).wait_send()

    @pl.loop(1, chain)
    def _(back):
        @pl.when(back <= spot)
        def _():
            mine = sp - 2 * back
            for group in range(2):

                @pl.when(spot < chain - 1)
                def _():
                    along(mine, group, stores[group].at[mine]).wait_send()

                across(mine, group, stores[group].at[mine]).wait_send()

    for step in range(1, tp_count):
        for group in range(2):
            spread(step, group).wait()


def attention(
    query_a, key_a, value_a, query_b, key_b, value_b, lambda_a, lambda_b, head_gain
):
    sp_count = lax.axis_size("sp")
    tp_count = lax.axis_size("tp")
    rows = query_a.shape[0]
    width = value_a.shape[2]

    def maps_of(query):
        flat = query[:, 0]
        size = flat.shape[1] // 2
        if size % 128 == 0:
            return jnp.stack([flat[:, :size], flat[:, size:]])
        first = jnp.arange(2 * size) < size
        zero = jnp.zeros_like(flat)
        return jnp.stack([jnp.where(first, flat, zero), jnp.where(first, zero, flat)])

    local_a = jnp.concatenate([key_a[:, 0], value_a[:, 0]], axis=1)
    local_b = jnp.concatenate([key_b[:, 0], value_b[:, 0]], axis=1)
    scalings = ((query_a.shape[2] // 2) ** (-0.5), (query_b.shape[2] // 2) ** (-0.5))
    vmem = pl.BlockSpec(memory_space=pltpu.VMEM)
    smem = pl.BlockSpec(memory_space=pltpu.SMEM)
    dma = pltpu.SemaphoreType.DMA
    return pl.pallas_call(
        functools.partial(attention_kernel, sp_count, tp_count, scalings),
        out_shape=jax.ShapeDtypeStruct((rows // tp_count, 2 * tp_count * width), jnp.bfloat16),
        in_specs=[vmem, vmem, vmem, vmem, smem, smem, vmem],
        out_specs=vmem,
        scratch_shapes=[
            pltpu.VMEM((sp_count,) + local_a.shape, jnp.bfloat16),
            pltpu.VMEM((sp_count,) + local_b.shape, jnp.bfloat16),
            pltpu.VMEM((4, rows, 128), jnp.float32),
            pltpu.VMEM((4, rows, 128), jnp.float32),
            pltpu.VMEM((4, rows, width), jnp.float32),
            pltpu.VMEM((rows, 2 * width), jnp.bfloat16),
            dma((sp_count, 2)),
            dma((sp_count, 2)),
            dma((sp_count, 2)),
            dma((tp_count, 2)),
            dma((tp_count, 2)),
        ],
        compiler_params=pltpu.CompilerParams(collective_id=0, has_side_effects=True),
        name="attention",
    )(
        maps_of(query_a),
        maps_of(query_b),
        local_a,
        local_b,
        lambda_a,
        lambda_b,
        head_gain[None, :],
    )


def per_device(
    resid,
    query_a,
    key_a,
    value_a,
    query_b,
    key_b,
    value_b,
    lambda_a,
    lambda_b,
    head_gain,
    out_weight,
    norm_gain,
    expert_ids,
    expert_mix,
    gate_experts,
    up_experts,
    down_experts,
    shared_gate,
    shared_up,
    shared_down,
):
    tok_dev = resid.shape[0]
    joined = attention(
        query_a, key_a, value_a, query_b, key_b, value_b, lambda_a, lambda_b, head_gain
    )
    project = jnp.dot(joined, out_weight, preferred_element_type=jnp.float32)
    middle = (resid.astype(jnp.float32) + project).astype(jnp.bfloat16)
    middle_f = middle.astype(jnp.float32)
    normed = (
        middle_f
        * lax.rsqrt(jnp.mean(middle_f * middle_f, axis=1, keepdims=True) + EPSILON)
        * norm_gain[None, :]
    ).astype(jnp.bfloat16)
    shared = swiglu_rows(normed, shared_gate, shared_up, shared_down)
    top_count = expert_ids.shape[1]
    model_width = normed.shape[1]
    sp_count = lax.axis_size("sp")
    tp_count = lax.axis_size("tp")
    expert_total = sp_count * tp_count
    pair_count = tok_dev * top_count
    capacity = max(2, 2 * pair_count // expert_total)
    hits = expert_ids[:, :, None] == jnp.arange(expert_total, dtype=jnp.int32)[None, None, :]
    named = jnp.any(hits, axis=1)
    mix_dense = jnp.sum(jnp.where(hits, expert_mix[:, :, None], 0.0), axis=1)
    counted = named.astype(jnp.int32)
    ranks = jnp.where(named, jnp.cumsum(counted, axis=0) - counted, -1)
    slots = jnp.arange(capacity, dtype=jnp.int32)
    placing = (ranks[:, :, None] == slots[None, None, :]).reshape(tok_dev, -1)
    send_rows = lax.dot_general(
        placing.astype(jnp.bfloat16),
        normed,
        (((0,), (0,)), ((), ())),
        preferred_element_type=jnp.float32,
    ).astype(jnp.bfloat16)
    send_rows = send_rows.reshape(expert_total, capacity, model_width)
    arrived = lax.all_to_all(send_rows, ("sp", "tp"), split_axis=0, concat_axis=0, tiled=True)
    arrived_shape = arrived.shape
    flat_rows = arrived.reshape(-1, arrived_shape[-1])
    result = swiglu_rows(flat_rows, gate_experts[0], up_experts[0], down_experts[0]).astype(
        jnp.bfloat16
    )
    finished = result.reshape(arrived_shape)
    returned = lax.all_to_all(finished, ("sp", "tp"), split_axis=0, concat_axis=0, tiled=True)
    flat_mix = jnp.broadcast_to(mix_dense[:, :, None], ranks.shape + (capacity,))
    weights = jnp.where(placing, flat_mix.reshape(tok_dev, -1), 0.0)
    coarse = lax.reduce_precision(weights, 8, 7)
    fine = weights - coarse
    flat_back = returned.reshape(-1, model_width)
    both = jnp.dot(
        jnp.concatenate([coarse, fine], axis=0).astype(jnp.bfloat16),
        flat_back,
        preferred_element_type=jnp.float32,
    )
    routed = both[:tok_dev] + both[tok_dev:]
    return (middle_f + shared + routed).astype(jnp.bfloat16)


def solution(mesh):
    in_specs = (
        P(("sp", "tp"), None),
        P("sp", "tp", None),
        P("sp", "tp", None),
        P("sp", "tp", None),
        P("sp", "tp", None),
        P("sp", "tp", None),
        P("sp", "tp", None),
        P("tp"),
        P("tp"),
        P(),
        P(),
        P(),
        P(("sp", "tp"), None),
        P(("sp", "tp"), None),
        P(("sp", "tp"), None, None),
        P(("sp", "tp"), None, None),
        P(("sp", "tp"), None, None),
        P(),
        P(),
        P(),
    )
    out_specs = P(("sp", "tp"), None)
    return jax.shard_map(
        per_device, mesh=mesh, in_specs=in_specs, out_specs=out_specs, check_vma=False
    )
```

time: 336 us -> 186 us (0.55)
  blocking collectives: 150 us -> 86.7 us
  local copies, waits for them, and re-layouts: 63.8 us -> 2.64 us
  between operations: 15.1 us -> 1.44 us
  Pallas kernels: 0 us -> 12.9 us
  waiting for transfers between devices: 53.1 us -> 46.4 us
  starting transfers between devices: 10.4 us -> 3.79 us
  matrix products: 33.6 us -> 27 us
    all_gather x3 -> x0, blocking collectives: 96.5 us -> none  [the longest x1 33.6 us: per_device(): key_piece_a = lax.all_gather(key_a, 'sp', axis=0, tiled=True)]
    scatter x1 -> x0, local copies, waits for them, and re-layouts: 46.2 us -> none  [per_device(): send_rows = jnp.zeros((expert_total, capacity, model_width), jnp.bfloat16...]
    all_to_all x1, blocking collectives: 53.7 us -> 86.7 us  [per_device(): lax.all_to_all(send_rows, ('sp', 'tp'), split_axis=0, concat_axis=0, tile...]
    pallas_call x0 -> x1, Pallas kernels: none -> 12.9 us  [attention(): pl.pallas_call(functools.partial(attention_kernel, sp_count, tp_count, sc...]
    gather x2 -> x0, local copies, waits for them, and re-layouts: 7.49 us -> none  [the longest x1 5.15 us: per_device(): returned[flat_ids, pair_rank].reshape(tok_dev, top_count, model_width)]
    dot_general x8 -> x2, matrix products: 10.9 us -> 3.87 us  [the longest x1 3.12 us: per_device(): jnp.dot(jnp.concatenate([coarse, fine], axis=0).astype(jnp.bfloat16), fla...]
    all_to_all x2 -> x0, starting transfers between devices: 6.57 us -> none  [the longest x1 3.28 us: per_device(): lax.all_to_all(heads_b, 'tp', split_axis=0, concat_axis=1, tiled=True)]
    all_to_all x2 -> x0, waiting for transfers between devices: 6.5 us -> none  [the longest x1 3.91 us: per_device(): lax.all_to_all(heads_a, 'tp', split_axis=0, concat_axis=1, tiled=True)]
  transfers between devices with their start and end apart: 4 -> 1, of which waited for: 3 -> 1; matrix products, arithmetic and copies ran while one was open for 3% -> 1% of each run, Pallas kernels for 0% -> 0%
where the time goes in v1:
time: 186 us
  blocking collectives  86.7 us (47%)
  waiting for transfers between devices  46.4 us (25%)
  matrix products  27 us (15%)
  Pallas kernels  12.9 us (7%)
  other arithmetic  5.21 us (3%)
  starting transfers between devices  3.79 us (2%)
  local copies, waits for them, and re-layouts  2.64 us (1%)
    all_to_all x1, blocking collectives, per_device(): lax.all_to_all(send_rows, ('sp', 'tp'), split_axis=0, concat_axis=0, tile...  86.7 us
    all_to_all x1, waiting for transfers between devices, per_device(): lax.all_to_all(finished, ('sp', 'tp'), split_axis=0, concat_axis=0, tiled...  46.4 us
    dot_general x2, matrix products, swiglu_rows(): return jnp.dot(hidden, w_down, preferred_element_type=jnp.float32)  14.1 us
    pallas_call x1, Pallas kernels, attention(): pl.pallas_call(functools.partial(attention_kernel, sp_count, tp_count, sc...  12.9 us
    dot_general x2, matrix products, swiglu_rows(): gate_val = jnp.dot(row_set, w_gate, preferred_element_type=jnp.float32)  5.77 us
    all_to_all x1, starting transfers between devices, per_device(): lax.all_to_all(finished, ('sp', 'tp'), split_axis=0, concat_axis=0, tiled...  3.79 us
  transfers between devices with their start and end apart: 1, of which 1 were waited for; matrix products, arithmetic and copies ran while one was open for 1% of the time, Pallas kernels for 0%

profile of v1, /device:TPU:0, one launch (start us, length us, event | category | flops | bytes accessed | tf_op | source)
XLA Modules:
  0.0 186.0 jit_solution(13885911101486134739)
XLA Ops:
  0.0 0.0 copy-start
  0.0 0.0 copy-start.2
  0.0 1.0 slice_bitcast_fusion.1
  2.4 0.9 bitcast_select_fusion.2
  3.2 1.6 pad_maximum_fusion.local_b
  4.9 1.6 pad_maximum_fusion.3.local_a
  6.4 0.7 pad_maximum_fusion.1
  7.1 12.9 %attention.1 = bf16[64,1024]{1,0:T(8,128)(2,1)} custom-call(bf16[2,256,128]{2,1,0:T(8,128)(2,1)} %get-tuple-element.13.query_a, bf16[2,256,128]{2,1,0:T(8,128)(2,1)} %get-tuple-element.14.query_b, bf16[256,256]{1,0:T(8,128)(2,1)} %pad_maximum_fusion.3.local_a, bf16[256,384]{1,0:T(8,128)(2,1)} %pad_maximum_fusion.local_b, f32[1]{0:T(128)S(6)} %copy.31.lam_a, ...), custom_call_target="tpu_custom_call" | custom-call | tf_op jit(solution)/shard_map/attention/pallas_call | solution.py:265
  20.0 0.0 copy-done.2
  20.0 0.0 copy-start.4
  20.0 0.0 copy-start.3
  20.0 3.2 %multiply_reduce_fusion = (f32[64]{0:T(128)S(1)}, f32[64,2048]{1,0:T(8,128)S(1)}) fusion(bf16[64,1024]{1,0:T(8,128)(2,1)} %attention.1, bf16[1024,2048]{1,0:T(8,128)(2,1)} %param.30, bf16[64,2048]{1,0:T(8,128)(2,1)S(1)} %copy-done.2), kind=kOutput, calls=%fused_computation.19 | convolution fusion | flops 269221824 | bytes 5112064 | tf_op jit(solution)/shard_map/dot_general | solution.py:322
  23.3 0.0 copy-done.4
  23.3 0.1 copy.27
  23.4 0.1 reduce_window_sum.11
  23.5 0.1 copy.28
  23.6 0.1 eq.39
  23.7 0.1 bitcast_compare_fusion
  23.9 0.0 copy-done.3
  23.9 0.8 convolution_convert_fusion
  24.6 0.0 copy-start.6
  24.6 86.7 %all_to_all.10 = bf16[32,16,2048]{2,1,0:T(8,128)(2,1)S(1)} all-to-all(bf16[32,16,2048]{2,1,0:T(8,128)(2,1)S(1)} %bitcast.53), channel_id=1, replica_groups=mesh['sp'=8,'tp'=4] {'sp','tp'}, dimensions={0} | all-to-all | bytes 4194304 | tf_op jit(solution)/shard_map/all_to_all | solution.py:352
  111.3 0.0 copy-start.1
  111.3 1.3 copy-done.1
  112.6 0.0 copy-done.6
  112.6 3.7 %fusion.4 = f32[512,1024]{1,0:T(8,128)} fusion(bf16[512,2048]{1,0:T(8,128)(2,1)S(1)} %bitcast.55, bf16[1,2048,1024]{2,1,0:T(8,128)(2,1)S(1)} %copy-done.6), kind=kOutput, calls=%fused_computation.4 | convolution fusion | flops 2147483648 | bytes 8388608 | tf_op jit(solution)/shard_map/dot_general | solution.py:18
  116.3 10.6 %fusion.6 = bf16[512,2048]{1,0:T(8,128)(2,1)} fusion(bf16[1,1024,2048]{2,1,0:T(8,128)(2,1)} %param.36, f32[512,1024]{1,0:T(8,128)} %fusion.4, bf16[512,2048]{1,0:T(8,128)(2,1)} %bitcast.56, bf16[1,2048,1024]{2,1,0:T(8,128)(2,1)} %param.35), kind=kOutput, calls=%fused_computation.6 | convolution fusion | flops 4299161600 | bytes 14680064 | tf_op jit(solution)/shard_map/dot_general | solution.py:21
  126.9 0.0 copy-start.5
  126.9 3.8 %all-to-all-start.1 = ((bf16[32,16,2048]{2,1,0:T(8,128)(2,1)}), bf16[32,16,2048]{2,1,0:T(8,128)(2,1)}, u32[]{:S(2)}, u32[]{:S(2)}) async-start(bf16[32,16,2048]{2,1,0:T(8,128)(2,1)} %bitcast.54), calls=%async_computation.1 | async-start | bytes 4194304 | tf_op jit(solution)/shard_map/all_to_all | solution.py:359
  130.7 0.0 copy-done.5
  130.7 0.1 reduce-precision_convert_fusion
  130.8 2.1 %fusion.33 = f32[64,512]{1,0:T(8,128)S(1)} fusion(bf16[2048,512]{1,0:T(8,128)(2,1)} %param.37, f32[64,2048]{1,0:T(8,128)S(1)} %get-tuple-element.12, f32[2048]{0:T(1024)S(1)} %copy-done.3, f32[64]{0:T(128)S(1)} %add_rsqrt_fusion), kind=kOutput, calls=%fused_computation.52 | convolution fusion | flops 134610944 | bytes 2760960 | tf_op jit(solution)/shard_map/dot_general | solution.py:18
  133.0 46.4 %all-to-all-done.1 = bf16[32,16,2048]{2,1,0:T(8,128)(2,1)} async-done(((bf16[32,16,2048]{2,1,0:T(8,128)(2,1)}), bf16[32,16,2048]{2,1,0:T(8,128)(2,1)}, u32[]{:S(2)}, u32[]{:S(2)}) %all-to-all-start.1) | async-done | bytes 2097184 | tf_op jit(solution)/shard_map/all_to_all | solution.py:359
  179.4 3.1 %fusion.19 = f32[128,2048]{1,0:T(8,128)} fusion(bf16[512,2048]{1,0:T(8,128)(2,1)} %bitcast.17, bf16[64,512]{0,1:T(8,128)(2,1)S(1)} %get-tuple-element.10, bf16[64,512]{0,1:T(8,128)(2,1)S(1)} %get-tuple-element.9), kind=kOutput, calls=%fused_computation.29 | convolution fusion | flops 268697600 | bytes 3276800 | tf_op jit(solution)/shard_map/dot_general | solution.py:365
  182.5 0.0 copy-done
  182.5 3.5 %fusion.10 = bf16[64,2048]{1,0:T(8,128)(2,1)} fusion(f32[64,2048]{1,0:T(8,128)S(1)} %get-tuple-element.12, bf16[512,2048]{1,0:T(8,128)(2,1)S(1)} %copy-done, bf16[2048,512]{1,0:T(8,128)(2,1)} %param.38, f32[128,2048]{1,0:T(8,128)} %fusion.19, f32[64,512]{1,0:T(8,128)S(1)} %fusion.33, f32[2048]{0:T(1024)S(1)} %copy-done.3, f32[64]{0:T(128)S(1)} %add_rsqrt_fusion), kind=kOutput, calls=%fused_computation.11 | convolution fusion | flops 269549568 | bytes 6693376 | tf_op jit(solution)/shard_map/dot_general | solution.py:21
  (7 shorter events, 0.1 us)
Async XLA Ops:
  0.0 182.5 %copy-start = (bf16[512,2048]{1,0:T(8,128)(2,1)S(1)}, bf16[512,2048]{1,0:T(8,128)(2,1)}, u32[]{:S(2)}) copy-start(bf16[512,2048]{1,0:T(8,128)(2,1)} %param.39) | copy-start | bytes 6291460
  0.0 20.0 %copy-start.2 = (bf16[64,2048]{1,0:T(8,128)(2,1)S(1)}, bf16[64,2048]{1,0:T(8,128)(2,1)}, u32[]{:S(2)}) copy-start(bf16[64,2048]{1,0:T(8,128)(2,1)} %param.20) | copy-start | bytes 786436
  20.0 3.3 %copy-start.4 = (s32[64,4]{0,1:T(4,128)S(1)}, s32[64,4]{0,1:T(4,128)}, u32[]{:S(2)}) copy-start(s32[64,4]{0,1:T(4,128)} %param.32) | copy-start | bytes 3076
  20.0 3.8 %copy-start.3 = (f32[2048]{0:T(1024)S(1)}, f32[2048]{0:T(1024)}, u32[]{:S(2)}) copy-start(f32[2048]{0:T(1024)} %param.31) | copy-start | bytes 24580
  24.6 88.0 %copy-start.6 = (bf16[1,2048,1024]{2,1,0:T(8,128)(2,1)S(1)}, bf16[1,2048,1024]{2,1,0:T(8,128)(2,1)}, u32[]{:S(2)}) copy-start(bf16[1,2048,1024]{2,1,0:T(8,128)(2,1)} %param.34) | copy-start | bytes 12582916
  111.3 1.3 copy-start.1
  126.9 3.8 %copy-start.5 = (f32[64,4]{0,1:T(4,128)S(1)}, f32[64,4]{0,1:T(4,128)}, u32[]{:S(2)}) copy-start(f32[64,4]{0,1:T(4,128)} %param.33) | copy-start | bytes 3076
  126.9 52.5 %all-to-all-start.1 = ((bf16[32,16,2048]{2,1,0:T(8,128)(2,1)}), bf16[32,16,2048]{2,1,0:T(8,128)(2,1)}, u32[]{:S(2)}, u32[]{:S(2)}) async-start(bf16[32,16,2048]{2,1,0:T(8,128)(2,1)} %bitcast.54), calls=%async_computation.1 | async-start | bytes 4194304 | tf_op jit(solution)/shard_map/all_to_all | solution.py:359

commit v2 on v1

--- a/solution.py
+++ b/solution.py
@@ -293,6 +293,313 @@
     )
 
 
+def plane_device(spot, member, tp_count):
+    return (spot * 2 + member // tp_count, member % tp_count)
+
+
+def expand_lanes(meta, first, members, capacity):
+    shape = (meta.shape[1], members * capacity)
+    column = lax.broadcasted_iota(jnp.int32, shape, 0)
+    lane = lax.broadcasted_iota(jnp.int32, shape, 1)
+    gap = lane - (column - first) * capacity
+    chosen = jnp.where((gap >= 0) & (gap < capacity), 1.0, 0.0).astype(jnp.bfloat16)
+    return jnp.dot(meta, chosen, preferred_element_type=jnp.float32)
+
+
+def dispatch_kernel(
+    sp_count,
+    tp_count,
+    model_width,
+    packed,
+    slot_at,
+    arrived,
+    metas,
+    held,
+    picks,
+    send_up,
+    send_down,
+    recv_z,
+    send_p,
+    recv_p,
+):
+    sp = lax.axis_index("sp")
+    tp = lax.axis_index("tp")
+    chain = sp_count // 2
+    members = 2 * tp_count
+    spot = sp // 2
+    member = (sp % 2) * tp_count + tp
+    capacity = arrived.shape[2]
+
+    barrier = pltpu.get_barrier_semaphore()
+
+    @pl.when(spot > 0)
+    def _():
+        pl.semaphore_signal(barrier, inc=1, device_id=(sp - 2, tp), device_id_type=MESH)
+
+    @pl.when(spot < chain - 1)
+    def _():
+        pl.semaphore_signal(barrier, inc=1, device_id=(sp + 2, tp), device_id_type=MESH)
+
+    for step in range(1, members):
+        peer = plane_device(spot, (member + step) % members, tp_count)
+        pl.semaphore_signal(barrier, inc=1, device_id=peer, device_id_type=MESH)
+    linked = jnp.where(spot > 0, 1, 0) + jnp.where(spot < chain - 1, 1, 0) + members - 1
+    pl.semaphore_wait(barrier, linked)
+
+    def move(block, source, shift, sems):
+        return pltpu.make_async_remote_copy(
+            src_ref=source,
+            dst_ref=held.at[block],
+            send_sem=sems.at[block],
+            recv_sem=recv_z.at[block],
+            device_id=(sp + 2 * shift, tp),
+            device_id_type=MESH,
+        )
+
+    def spread(block, step):
+        target = (member + step) % members
+        return pltpu.make_async_remote_copy(
+            src_ref=picks.at[block, target],
+            dst_ref=arrived.at[block, member],
+            send_sem=send_p.at[block, step],
+            recv_sem=recv_p.at[block, step],
+            device_id=plane_device(spot, target, tp_count),
+            device_id_type=MESH,
+        )
+
+    def place(block, source):
+        meta = source[:, model_width:]
+        metas[block] = meta
+        ranks = expand_lanes(meta, spot * members, members, capacity)
+        placing = jnp.where(ranks == slot_at[...], 1.0, 0.0).astype(jnp.bfloat16)
+        rows = lax.dot_general(
+            placing,
+            source[:, :model_width],
+            (((0,), (0,)), ((), ())),
+            preferred_element_type=jnp.float32,
+        )
+        for index in range(members):
+            picks[block, index] = rows[index * capacity : (index + 1) * capacity].astype(
+                jnp.bfloat16
+            )
+        for step in range(1, members):
+            spread(block, step).start()
+        arrived[block, member] = picks[block, member]
+
+    @pl.when(spot < chain - 1)
+    def _():
+        move(spot, packed, 1, send_up).start()
+
+    @pl.when(spot > 0)
+    def _():
+        move(spot, packed, -1, send_down).start()
+
+    place(spot, packed)
+
+    @pl.loop(1, chain)
+    def _(back):
+        low = spot - back
+        high = spot + back
+
+        @pl.when(low >= 0)
+        def _():
+            move(low, held.at[low], 1, send_up).wait_recv()
+
+            @pl.when(spot < chain - 1)
+            def _():
+                move(low, held.at[low], 1, send_up).start()
+
+        @pl.when(high < chain)
+        def _():
+            move(high, held.at[high], -1, send_down).wait_recv()
+
+            @pl.when(spot > 0)
+            def _():
+                move(high, held.at[high], -1, send_down).start()
+
+        @pl.when(low >= 0)
+        def _():
+            place(low, held.at[low])
+
+        @pl.when(high < chain)
+        def _():
+            place(high, held.at[high])
+
+    @pl.when(spot < chain - 1)
+    def _():
+        move(spot, packed, 1, send_up).wait_send()
+
+    @pl.when(spot > 0)
+    def _():
+        move(spot, packed, -1, send_down).wait_send()
+
+    @pl.loop(1, chain)
+    def _(back):
+        low = spot - back
+        high = spot + back
+
+        @pl.when((low >= 0) & (spot < chain - 1))
+        def _():
+            move(low, held.at[low], 1, send_up).wait_send()
+
+        @pl.when((high < chain) & (spot > 0))
+        def _():
+            move(high, held.at[high], -1, send_down).wait_send()
+
+    @pl.loop(0, chain)
+    def _(block):
+        for step in range(1, members):
+            spread(block, step).wait()
+
+
+def return_kernel(
+    sp_count,
+    tp_count,
+    expert_total,
+    finished,
+    metas,
+    slot_at,
+    middle,
+    normed,
+    gate,
+    up,
+    down,
+    out,
+    back,
+    part_out,
+    part_in,
+    total,
+    send_p,
+    recv_p,
+    send_z,
+    recv_z,
+):
+    sp = lax.axis_index("sp")
+    tp = lax.axis_index("tp")
+    chain = sp_count // 2
+    members = 2 * tp_count
+    spot = sp // 2
+    side = sp % 2
+    member = side * tp_count + tp
+    capacity = finished.shape[2]
+
+    barrier = pltpu.get_barrier_semaphore()
+    for step in range(1, members):
+        peer = plane_device(spot, (member + step) % members, tp_count)
+        pl.semaphore_signal(barrier, inc=1, device_id=peer, device_id_type=MESH)
+    for step in range(1, chain):
+        peer = (((spot + step) % chain) * 2 + side, tp)
+        pl.semaphore_signal(barrier, inc=1, device_id=peer, device_id_type=MESH)
+    pl.semaphore_wait(barrier, members + chain - 2)
+
+    def spread(block, step):
+        target = (member + step) % members
+        return pltpu.make_async_remote_copy(
+            src_ref=finished.at[block, target],
+            dst_ref=back.at[block, member],
+            send_sem=send_p.at[block, step],
+            recv_sem=recv_p.at[block, step],
+            device_id=plane_device(spot, target, tp_count),
+            device_id_type=MESH,
+        )
+
+    def deliver(block):
+        return pltpu.make_async_remote_copy(
+            src_ref=part_out.at[block],
+            dst_ref=part_in.at[spot],
+            send_sem=send_z.at[block],
+            recv_sem=recv_z.at[spot],
+            device_id=(block * 2 + side, tp),
+            device_id_type=MESH,
+        )
+
+    def collect(block):
+        return pltpu.make_async_remote_copy(
+            src_ref=part_out.at[block],
+            dst_ref=part_in.at[block],
+            send_sem=send_z.at[block],
+            recv_sem=recv_z.at[block],
+            device_id=(block * 2 + side, tp),
+            device_id_type=MESH,
+        )
+
+    def far_first(body):
+        @pl.loop(0, 2 * chain)
+        def _(turn):
+            away = chain - 1 - turn // 2
+            block = spot + away * (1 - 2 * (turn % 2))
+
+            @pl.when((block >= 0) & (block < chain) & ((away > 0) | (turn % 2 == 0)))
+            def _():
+                body(block)
+
+    def start_spread(block):
+        for step in range(1, members):
+            spread(block, step).start()
+        back[block, member] = finished[block, member]
+
+    far_first(start_spread)
+
+    rows = normed[...]
+    gate_val = jnp.dot(rows, gate[...], preferred_element_type=jnp.float32)
+    up_val = jnp.dot(rows, up[...], preferred_element_type=jnp.float32)
+    hidden = (jax.nn.silu(gate_val) * up_val).astype(jnp.bfloat16)
+    total[...] = middle[...].astype(jnp.float32) + jnp.dot(
+        hidden, down[...], preferred_element_type=jnp.float32
+    )
+
+    def mix(block):
+        for step in range(1, members):
+            spread(block, step).wait_recv()
+        meta = metas[block]
+        first = spot * members
+        ranks = expand_lanes(meta, first, members, capacity)
+        coarse = expand_lanes(meta, first + expert_total, members, capacity)
+        fine = expand_lanes(meta, first + 2 * expert_total, members, capacity)
+        placed = ranks == slot_at[...]
+        weights = jnp.concatenate(
+            [jnp.where(placed, coarse, 0.0), jnp.where(placed, fine, 0.0)], axis=0
+        ).astype(jnp.bfloat16)
+        if capacity % 16 == 0:
+            slots = back[block].reshape(members * capacity, back.shape[3])
+        else:
+            slots = jnp.concatenate(
+                [back[block, index].astype(jnp.float32) for index in range(members)], axis=0
+            ).astype(jnp.bfloat16)
+        both = jnp.dot(weights, slots, preferred_element_type=jnp.float32)
+        tokens = meta.shape[0]
+        sums = both[:tokens] + both[tokens:]
+
+        @pl.when(block == spot)
+        def _():
+            total[...] += sums
+
+        @pl.when(block != spot)
+        def _():
+            part_out[block] = sums.astype(jnp.bfloat16)
+            deliver(block).start()
+
+    far_first(mix)
+
+    @pl.loop(1, chain)
+    def _(step):
+        block = (spot + step) % chain
+        collect(block).wait_recv()
+        total[...] += part_in[block].astype(jnp.float32)
+
+    out[...] = total[...].astype(jnp.bfloat16)
+
+    @pl.loop(1, chain)
+    def _(step):
+        block = (spot + step) % chain
+        deliver(block).wait_send()
+
+    @pl.loop(0, chain)
+    def _(block):
+        for step in range(1, members):
+            spread(block, step).wait_send()
+
+
 def per_device(
     resid,
     query_a,
@@ -327,7 +634,6 @@
         * lax.rsqrt(jnp.mean(middle_f * middle_f, axis=1, keepdims=True) + EPSILON)
         * norm_gain[None, :]
     ).astype(jnp.bfloat16)
-    shared = swiglu_rows(normed, shared_gate, shared_up, shared_down)
     top_count = expert_ids.shape[1]
     model_width = normed.shape[1]
     sp_count = lax.axis_size("sp")
@@ -340,35 +646,68 @@
     mix_dense = jnp.sum(jnp.where(hits, expert_mix[:, :, None], 0.0), axis=1)
     counted = named.astype(jnp.int32)
     ranks = jnp.where(named, jnp.cumsum(counted, axis=0) - counted, -1)
-    slots = jnp.arange(capacity, dtype=jnp.int32)
-    placing = (ranks[:, :, None] == slots[None, None, :]).reshape(tok_dev, -1)
-    send_rows = lax.dot_general(
-        placing.astype(jnp.bfloat16),
-        normed,
-        (((0,), (0,)), ((), ())),
-        preferred_element_type=jnp.float32,
-    ).astype(jnp.bfloat16)
-    send_rows = send_rows.reshape(expert_total, capacity, model_width)
-    arrived = lax.all_to_all(send_rows, ("sp", "tp"), split_axis=0, concat_axis=0, tiled=True)
-    arrived_shape = arrived.shape
-    flat_rows = arrived.reshape(-1, arrived_shape[-1])
+    coarse = lax.reduce_precision(mix_dense, 8, 7)
+    meta = jnp.concatenate([ranks.astype(jnp.float32), coarse, mix_dense - coarse], axis=1)
+    spare = -meta.shape[1] % 128
+    meta = jnp.pad(meta, ((0, 0), (0, spare))).astype(jnp.bfloat16)
+    packed = jnp.concatenate([normed, meta], axis=1)
+    members = 2 * tp_count
+    chain = sp_count // 2
+    slot_at = jnp.tile(jnp.arange(capacity, dtype=jnp.float32), members)[None, :]
+    vmem = pl.BlockSpec(memory_space=pltpu.VMEM)
+    dma = pltpu.SemaphoreType.DMA
+    slot_shape = (chain, members, capacity, model_width)
+    arrived, metas = pl.pallas_call(
+        functools.partial(dispatch_kernel, sp_count, tp_count, model_width),
+        out_shape=(
+            jax.ShapeDtypeStruct(slot_shape, jnp.bfloat16),
+            jax.ShapeDtypeStruct((chain,) + meta.shape, jnp.bfloat16),
+        ),
+        in_specs=[vmem, vmem],
+        out_specs=(vmem, vmem),
+        scratch_shapes=[
+            pltpu.VMEM((chain,) + packed.shape, jnp.bfloat16),
+            pltpu.VMEM(slot_shape, jnp.bfloat16),
+            dma((chain,)),
+            dma((chain,)),
+            dma((chain,)),
+            dma((chain, members)),
+            dma((chain, members)),
+        ],
+        compiler_params=pltpu.CompilerParams(collective_id=1, has_side_effects=True),
+        name="dispatch",
+    )(packed, slot_at)
+    flat_rows = arrived.reshape(-1, model_width)
     result = swiglu_rows(flat_rows, gate_experts[0], up_experts[0], down_experts[0]).astype(
         jnp.bfloat16
     )
-    finished = result.reshape(arrived_shape)
-    returned = lax.all_to_all(finished, ("sp", "tp"), split_axis=0, concat_axis=0, tiled=True)
-    flat_mix = jnp.broadcast_to(mix_dense[:, :, None], ranks.shape + (capacity,))
-    weights = jnp.where(placing, flat_mix.reshape(tok_dev, -1), 0.0)
-    coarse = lax.reduce_precision(weights, 8, 7)
-    fine = weights - coarse
-    flat_back = returned.reshape(-1, model_width)
-    both = jnp.dot(
-        jnp.concatenate([coarse, fine], axis=0).astype(jnp.bfloat16),
-        flat_back,
-        preferred_element_type=jnp.float32,
+    return pl.pallas_call(
+        functools.partial(return_kernel, sp_count, tp_count, expert_total),
+        out_shape=jax.ShapeDtypeStruct((tok_dev, model_width), jnp.bfloat16),
+        in_specs=[vmem] * 8,
+        out_specs=vmem,
+        scratch_shapes=[
+            pltpu.VMEM(slot_shape, jnp.bfloat16),
+            pltpu.VMEM((chain, tok_dev, model_width), jnp.bfloat16),
+            pltpu.VMEM((chain, tok_dev, model_width), jnp.bfloat16),
+            pltpu.VMEM((tok_dev, model_width), jnp.float32),
+            dma((chain, members)),
+            dma((chain, members)),
+            dma((chain,)),
+            dma((chain,)),
+        ],
+        compiler_params=pltpu.CompilerParams(collective_id=2, has_side_effects=True),
+        name="give_back",
+    )(
+        result.reshape(slot_shape),
+        metas,
+        slot_at,
+        middle,
+        normed,
+        shared_gate,
+        shared_up,
+        shared_down,
     )
-    routed = both[:tok_dev] + both[tok_dev:]
-    return (middle_f + shared + routed).astype(jnp.bfloat16)
 
 
 def solution(mesh):

time: 186 us -> 151 us (0.81)
  Pallas kernels: 12.9 us -> 118 us
  blocking collectives: 86.7 us -> 0 us
  waiting for transfers between devices: 46.4 us -> 0 us
  matrix products: 27 us -> 19.8 us
  starting transfers between devices: 3.79 us -> 0 us
  other arithmetic: 5.21 us -> 7.34 us
    pallas_call x0 -> x2, Pallas kernels: none -> 105 us  [the longest x1 67.7 us: per_device(): pl.pallas_call(functools.partial(dispatch_kernel, sp_count, tp_count, mod...]
    all_to_all x1 -> x0, blocking collectives: 86.7 us -> none  [per_device(): lax.all_to_all(send_rows, ('sp', 'tp'), split_axis=0, concat_axis=0, tile...]
    all_to_all x1 -> x0, waiting for transfers between devices: 46.4 us -> none  [per_device(): lax.all_to_all(finished, ('sp', 'tp'), split_axis=0, concat_axis=0, tiled...]
    dot_general x2 -> x1, matrix products: 14.1 us -> 9.96 us  [swiglu_rows(): return jnp.dot(hidden, w_down, preferred_element_type=jnp.float32)]
    dot_general x2 -> x0, matrix products: 3.87 us -> none  [the longest x1 3.12 us: per_device(): jnp.dot(jnp.concatenate([coarse, fine], axis=0).astype(jnp.bfloat16), fla...]
    all_to_all x1 -> x0, starting transfers between devices: 3.79 us -> none  [per_device(): lax.all_to_all(finished, ('sp', 'tp'), split_axis=0, concat_axis=0, tiled...]
    dot_general x2 -> x1, matrix products: 5.77 us -> 6.59 us  [swiglu_rows(): gate_val = jnp.dot(row_set, w_gate, preferred_element_type=jnp.float32)]
  transfers between devices with their start and end apart: 1 -> 0, of which waited for: 1 -> 0; matrix products, arithmetic and copies ran while one was open for 1% -> 0% of each run, Pallas kernels for 0% -> 0%
where the time goes in v2:
time: 151 us; the launch traced here: 150 us
  Pallas kernels  118 us (78%)
  matrix products  19.8 us (13%)
  other arithmetic  7.34 us (5%)
  local copies, waits for them, and re-layouts  3.46 us (2%)
    pallas_call x1, Pallas kernels, per_device(): pl.pallas_call(functools.partial(dispatch_kernel, sp_count, tp_count, mod...  67.7 us
    pallas_call x1, Pallas kernels, per_device(): pl.pallas_call(functools.partial(return_kernel, sp_count, tp_count, exper...  37.3 us
    pallas_call x1, Pallas kernels, attention(): pl.pallas_call(functools.partial(attention_kernel, sp_count, tp_count, sc...  12.9 us
    dot_general x1, matrix products, swiglu_rows(): return jnp.dot(hidden, w_down, preferred_element_type=jnp.float32)  9.96 us
    dot_general x1, matrix products, swiglu_rows(): gate_val = jnp.dot(row_set, w_gate, preferred_element_type=jnp.float32)  6.59 us
    dot_general x1, matrix products, per_device(): project = jnp.dot(joined, out_weight, preferred_element_type=jnp.float32)  3.24 us

profile of v2, /device:TPU:0, one launch (start us, length us, event | category | flops | bytes accessed | tf_op | source)
XLA Modules:
  0.0 150.0 jit_solution(4684845365690176883)
XLA Ops:
  0.0 0.0 copy-start.2
  1.4 0.7 fusion.17
  2.1 0.1 copy.28
  2.2 0.6 broadcast_in_dim_tile.5.slot_at
  2.8 0.7 select_reduce_fusion
  3.5 0.1 copy.30
  3.6 0.1 copy.29
  3.7 0.1 reduce_window_sum.11
  3.8 0.1 fusion.22
  3.9 0.9 bitcast_select_fusion.1
  4.8 1.5 %pad_maximum_fusion.4.local_a = bf16[256,256]{1,0:T(8,128)(2,1)} fusion(bf16[256,128]{1,0:T(8,128)(2,1)} %bitcast.37, bf16[256,128]{1,0:T(8,128)(2,1)} %bitcast.38), kind=kLoop, calls=%fused_computation.19 | loop fusion | flops 262144 | bytes 262144 | tf_op jit(solution)/shard_map/concatenate | solution.py:259
  6.3 0.9 slice_bitcast_fusion.1
  7.2 0.7 pad_maximum_fusion.2
  7.9 1.6 %pad_maximum_fusion.1.local_b = bf16[256,384]{1,0:T(8,128)(2,1)} fusion(bf16[256,128]{1,0:T(8,128)(2,1)} %bitcast.39, bf16[256,256]{1,0:T(8,128)(2,1)} %bitcast.35), kind=kLoop, calls=%fused_computation.16 | loop fusion | flops 393216 | bytes 393216 | tf_op jit(solution)/shard_map/concatenate | solution.py:260
  9.6 12.9 %attention.1 = bf16[64,1024]{1,0:T(8,128)(2,1)} custom-call(bf16[2,256,128]{2,1,0:T(8,128)(2,1)} %get-tuple-element.17.query_a, bf16[2,256,128]{2,1,0:T(8,128)(2,1)} %get-tuple-element.18.query_b, bf16[256,256]{1,0:T(8,128)(2,1)} %pad_maximum_fusion.4.local_a, bf16[256,384]{1,0:T(8,128)(2,1)} %pad_maximum_fusion.1.local_b, f32[1]{0:T(128)S(6)} %copy.33.lam_a, ...), custom_call_target="tpu_custom_call" | custom-call | tf_op jit(solution)/shard_map/attention/pallas_call | solution.py:265
  22.4 0.0 copy-done.2
  22.4 0.0 copy-start.3
  22.5 3.2 %fusion.14 = (f32[64]{0:T(128)S(1)}, bf16[64,2048]{1,0:T(8,128)(2,1)S(1)}) fusion(bf16[64,1024]{1,0:T(8,128)(2,1)} %attention.1, bf16[1024,2048]{1,0:T(8,128)(2,1)} %param.30, bf16[64,2048]{1,0:T(8,128)(2,1)S(1)} %copy-done.2), kind=kOutput, calls=%fused_computation.12 | convolution fusion | flops 269221824 | bytes 4849920 | tf_op jit(solution)/shard_map/dot_general | solution.py:629
  25.7 0.0 copy-start
  25.7 0.0 copy-done.3
  25.7 0.1 fusion.16.normed
  25.9 0.0 copy-start.1
  25.9 0.8 pad_maximum_fusion.packed
  26.7 67.7 %dispatch.1 = (bf16[4,8,16,2048]{3,2,1,0:T(8,128)(2,1)}, bf16[4,64,128]{2,1,0:T(8,128)(2,1)}) custom-call(bf16[64,2176]{1,0:T(8,128)(2,1)} %pad_maximum_fusion.packed, f32[1,128]{1,0:T(1,128)} %broadcast_in_dim_tile.5.slot_at), custom_call_target="tpu_custom_call" | custom-call | tf_op jit(solution)/shard_map/dispatch/pallas_call | solution.py:660
  94.4 0.0 copy-start.4
  94.4 6.6 %fusion.4 = f32[512,1024]{1,0:T(8,128)} fusion(bf16[512,2048]{1,0:T(8,128)(2,1)} %bitcast.41, bf16[1,2048,1024]{2,1,0:T(8,128)(2,1)} %param.34), kind=kOutput, calls=%fused_computation.4 | convolution fusion | flops 2147483648 | bytes 8388608 | tf_op jit(solution)/shard_map/dot_general | solution.py:18
  101.0 0.0 copy-done
  101.0 0.0 copy-done.1
  101.0 0.0 copy-done.4
  101.0 10.0 %fusion.6 = bf16[512,2048]{1,0:T(8,128)(2,1)} fusion(bf16[1,1024,2048]{2,1,0:T(8,128)(2,1)} %param.36, f32[512,1024]{1,0:T(8,128)} %fusion.4, bf16[512,2048]{1,0:T(8,128)(2,1)S(1)} %bitcast.42, bf16[1,2048,1024]{2,1,0:T(8,128)(2,1)} %param.35), kind=kOutput, calls=%fused_computation.6 | convolution fusion | flops 4299161600 | bytes 14680064 | tf_op jit(solution)/shard_map/dot_general | solution.py:21
  111.0 37.3 %give_back.1 = bf16[64,2048]{1,0:T(8,128)(2,1)} custom-call(bf16[4,8,16,2048]{3,2,1,0:T(8,128)(2,1)} %bitcast.34, bf16[4,64,128]{2,1,0:T(8,128)(2,1)} %get-tuple-element.8.metas, f32[1,128]{1,0:T(1,128)} %broadcast_in_dim_tile.5.slot_at, bf16[64,2048]{1,0:T(8,128)(2,1)} %copy-done, bf16[64,2048]{1,0:T(8,128)(2,1)} %copy-done.1, bf16[2048,512]{1,0:T(8,128)(2,1)} %gate.1, ...), custom_call_target="tpu_custom_call" | custom-call | tf_op jit(solution)/shard_map/give_back/pallas_call | solution.py:684
  148.3 1.7 %copy.35 = bf16[64,2048]{1,0:T(8,128)(2,1)} copy(bf16[64,2048]{1,0:T(8,128)(2,1)} %give_back.1) | data formatting | bytes 524288
  (7 shorter events, 0.1 us)
Async XLA Ops:
  0.0 22.4 %copy-start.2 = (bf16[64,2048]{1,0:T(8,128)(2,1)S(1)}, bf16[64,2048]{1,0:T(8,128)(2,1)}, u32[]{:S(2)}) copy-start(bf16[64,2048]{1,0:T(8,128)(2,1)} %param.20) | copy-start | bytes 786436
  22.4 3.3 %copy-start.3 = (f32[2048]{0:T(1024)S(1)}, f32[2048]{0:T(1024)}, u32[]{:S(2)}) copy-start(f32[2048]{0:T(1024)} %param.31) | copy-start | bytes 24580
  25.7 75.3 %copy-start = (bf16[64,2048]{1,0:T(8,128)(2,1)}, bf16[64,2048]{1,0:T(8,128)(2,1)S(1)}, u32[]{:S(2)}) copy-start(bf16[64,2048]{1,0:T(8,128)(2,1)S(1)} %get-tuple-element.16.middle) | copy-start | bytes 786436
  25.9 75.1 %copy-start.1 = (bf16[64,2048]{1,0:T(8,128)(2,1)}, bf16[64,2048]{1,0:T(8,128)(2,1)S(1)}, u32[]{:S(2)}) copy-start(bf16[64,2048]{1,0:T(8,128)(2,1)S(1)} %fusion.16.normed) | copy-start | bytes 786436
  94.4 6.6 %copy-start.4 = (bf16[4,8,16,2048]{3,2,1,0:T(8,128)(2,1)S(1)}, bf16[4,8,16,2048]{3,2,1,0:T(8,128)(2,1)}, u32[]{:S(2)}) copy-start(bf16[4,8,16,2048]{3,2,1,0:T(8,128)(2,1)} %get-tuple-element.7) | copy-start | bytes 6291460
